TPU v7x, 256 devices: a whole 4x4x8 slice. The times are simulated.
256 devices in a mesh: sp: 32 (over z, y), fs: 4 (over x), tp: 2 (over core).
Axes of the slice: x: 4, y: 4, z: 8, core: 2. Of those that a mesh axis runs over, the one named last changes fastest.
Arguments:
- tokens: bfloat16 [16384, 2048], P(('fs', 'sp'), 'tp'), parts along dimension 0, may hold values from -6 to 6
- norm_gain: float32 [2048], replicated, may hold values from 0.1 to 1.9
- w_recur_in: bfloat16 [2048, 1024], P(None, 'tp'), may hold values from -0.125 to 0.125
- conv_weight: float32 [4, 1024], P(None, 'tp'), may hold values from -3 to 3
- w_gate_decay: bfloat16 [16, 64, 64], P('tp'), may hold values from -0.75 to 0.75
- w_gate_input: bfloat16 [16, 64, 64], P('tp'), may hold values from -0.75 to 0.75
- decay_base: float32 [1024], P('tp'), may hold values from 0 to 0.01, as said below
- extra_decay: float32 [16384, 16], P(('fs', 'sp'), 'tp'), parts along dimension 0, may hold values from 0 to 1, as said below
- w_query: bfloat16 [2048, 1024], P(None, 'tp'), may hold values from -1 to 1
- w_key: bfloat16 [2048, 256], P(None, 'tp'), may hold values from -20 to 20
- w_value: bfloat16 [2048, 256], P(None, 'tp'), may hold values from -0.125 to 0.125
- mix_lambda: float32 [8], P('tp'), may hold values from 0.3 to 0.8
- head_gain: float32 [128], replicated, may hold values from 0.1 to 1.9
- w_out_recur: bfloat16 [1024, 2048], P('tp'), may hold values from -0.125 to 0.125
- w_out_attend: bfloat16 [1024, 2048], P('tp'), may hold values from -0.125 to 0.125
- out_gain: float32 [2048], replicated, may hold values from 0.1 to 1.9
Outputs:
- mixed: bfloat16 [16384, 2048], P(('fs', 'sp', 'tp')), parts along dimension 0
There are 4 independent parts, one for each index of `fs`. A program takes and returns all parts, laid end to end along the dimension named above; an argument that names none is the same for every part. Nothing has to cross between parts.
Inputs may be any that keep to these rules, and one draw needn't show every extreme that they name: `decay_base`: positive rates of each channel. `extra_decay`: non-negative added log-decays.
All inputs are finite; a program needn't handle non-finite values.
Results may differ from a plain program's by a relative error of at most 0.012.
The roundings to bfloat16 on the way count: a program that leaves them out, or rounds other values in their place, can miss the bound.
Values may be sent and summed in bfloat16 or wider, within the bound.
A program may use at most 128 MiB of HBM per device.

v0:
```python
import jax
import jax.numpy as jnp
from jax import lax
from jax.sharding import PartitionSpec as P

D = 2048
HEAD = 64
DV = 128
lru_rate = 8.0
norm_eps = 1e-06


def shifted(block, axis, distance):
    devices = range(lax.axis_size(axis))
    route = [(i - distance, i) for i in devices if i - distance in devices]
    return lax.ppermute(block, axis, route)


def copy_for_each(shard, axis):
    copies = jnp.broadcast_to(shard, (lax.axis_size(axis), *shard.shape))
    return lax.all_to_all(copies, axis, split_axis=0, concat_axis=0, tiled=True)


def all_in_one(shard, axis):
    leaves = jax.tree.leaves(shard)
    sequence = sorted(range(len(leaves)), key=lambda k: -leaves[k].size)
    width = (1, *leaves[sequence[0]].shape)[-1]
    lines = [
        jnp.pad(leaves[k].reshape(-1), (0, -leaves[k].size % width)).reshape(-1, width)
        for k in sequence
    ]
    both, at, found = (copy_for_each(jnp.concatenate(lines), axis), 0, {})
    for k, line in zip(sequence, lines):
        share = both[:, at : at + len(line)].reshape(len(both), -1)
        found[k] = share[:, : leaves[k].size].reshape(-1, *leaves[k].shape)
        at += len(line)
    numbers = iter(range(len(leaves)))
    return jax.tree.map(lambda _: found[next(numbers)], shard)


def folded_in_pairs(pieces, combine):
    while len(jax.tree.leaves(pieces)[0]) > 1:
        pieces = jax.vmap(combine)(
            *(jax.tree.map(lambda part: part[side::2], pieces) for side in (0, 1))
        )
    return jax.tree.map(lambda part: part[0], pieces)


def carried_in(shard, axis, combine, identity):
    length, index = (lax.axis_size(axis), lax.axis_index(axis))
    passed = jnp.arange(length) < index

    def kept(part, zero, own):
        part = jnp.where(
            passed.reshape(-1, *(1 for _ in own.shape)), part, jnp.asarray(zero, own.dtype)
        )
        return part

    pieces = all_in_one(shard, axis)
    return folded_in_pairs(jax.tree.map(kept, pieces, identity, shard), combine)


def in_one_piece(arrays, axis, dim, along):
    both = jnp.concatenate(arrays, axis=along)
    result, at, outs = (lax.all_gather(both, axis, axis=dim, tiled=True), 0, [])
    for a in arrays:
        outs.append(lax.slice_in_dim(result, at, at + a.shape[along], axis=along))
        at += a.shape[along]
    return tuple(outs)


def chain(earlier, later):
    return (earlier[0] * later[0], later[0] * earlier[1] + later[1])


def body(
    tokens,
    norm_gain,
    w_recur_in,
    conv_weight,
    w_gate_decay,
    w_gate_input,
    decay_base,
    extra_decay,
    w_query,
    w_key,
    w_value,
    mix_lambda,
    head_gain,
    w_out_recur,
    w_out_attend,
    out_gain,
):
    row_count = tokens.shape[0]
    recur_cols = w_recur_in.shape[1]
    query_cols = w_query.shape[1]
    key_cols = w_key.shape[1]
    all_weights = jnp.concatenate([w_recur_in, w_query, w_key, w_value], axis=1)
    wide_piece = lax.all_gather(tokens, "tp", axis=1, tiled=True).astype(jnp.float32)
    scaled = (wide_piece * norm_gain).astype(jnp.bfloat16)
    accum = jnp.dot(scaled, all_weights, preferred_element_type=jnp.float32)
    squares = jnp.sum(wide_piece * wide_piece, axis=1, keepdims=True)
    accum, squares = (accum, squares)
    inverse = lax.rsqrt(squares / D + norm_eps)
    projected = (accum * inverse).astype(jnp.bfloat16)
    recur_in = projected[:, :recur_cols]
    queries = projected[:, recur_cols : recur_cols + query_cols]
    keys = projected[:, recur_cols + query_cols : recur_cols + query_cols + key_cols]
    values = projected[:, recur_cols + query_cols + key_cols :]
    taps = conv_weight.shape[0]
    carried_rows = shifted(recur_in[row_count - (taps - 1) :], "sp", 1)
    padded = jnp.concatenate([carried_rows, recur_in], axis=0).astype(jnp.float32)
    conv_acc = jnp.zeros((row_count, recur_cols), jnp.float32)
    for offset in range(taps):
        conv_acc = conv_acc + conv_weight[offset] * padded[offset : offset + row_count]
    conv_in = conv_acc.astype(jnp.bfloat16)
    gate_blocks = w_gate_decay.shape[0]
    blocks = conv_in.reshape(row_count, gate_blocks, HEAD)
    decay_gate = jax.nn.sigmoid(
        jnp.einsum("thi,hij->thj", blocks, w_gate_decay, preferred_element_type=jnp.float32)
    ).reshape(row_count, recur_cols)
    input_gate = jax.nn.sigmoid(
        jnp.einsum("thi,hij->thj", blocks, w_gate_input, preferred_element_type=jnp.float32)
    ).reshape(row_count, recur_cols)
    log_decay = -lru_rate * decay_gate * decay_base - jnp.repeat(extra_decay, HEAD, axis=1)
    decay = jnp.exp(log_decay)
    inject = jnp.sqrt(-jnp.expm1(2.0 * log_decay)) * input_gate * conv_in.astype(jnp.float32)
    decay_cum, local_state = lax.associative_scan(chain, (decay, inject), axis=0)
    identity = (jnp.ones((recur_cols,), jnp.float32), jnp.zeros((recur_cols,), jnp.float32))
    carried = carried_in(
        (decay_cum[row_count - 1], local_state[row_count - 1]), "sp", chain, identity
    )
    recur_out = (local_state + decay_cum * carried[1]).astype(jnp.bfloat16)
    kv_local = key_cols // (2 * HEAD)
    heads_local = query_cols // (2 * HEAD)
    group_size = heads_local // kv_local
    local_query = queries.reshape(row_count, kv_local, group_size, 2, HEAD)
    offset_rows = lax.axis_index("sp") * row_count
    positions = offset_rows + jnp.arange(row_count, dtype=jnp.int32)
    last_position = offset_rows + row_count - 1
    lambdas = mix_lambda.reshape(kv_local, group_size)
    start_state = (
        jnp.full((2, kv_local, group_size, row_count), -1e30, jnp.float32),
        jnp.zeros((2, kv_local, group_size, row_count), jnp.float32),
        jnp.zeros((2, row_count, kv_local, group_size, DV), jnp.float32),
    )
    key_piece, value_piece = in_one_piece((keys, values), "sp", 0, 1)
    count = key_piece.shape[0]

    def update(state):
        peaks, totals, attends = state
        key_three = key_piece.reshape(count, kv_local, 2, HEAD)
        value_three = value_piece.reshape(count, kv_local, DV)
        allowed = positions[:, None] >= jnp.arange(count, dtype=jnp.int32)[None, :]
        new_peaks, new_totals, new_attends = ([], [], [])
        for mapping in range(2):
            scores = jnp.einsum(
                "bkgd,tkd->kgbt",
                local_query[:, :, :, mapping, :],
                key_three[:, :, mapping, :],
                preferred_element_type=jnp.float32,
            ) * HEAD ** (-0.5)
            scores = jnp.where(allowed, scores, -jnp.inf)
            peak = jnp.maximum(peaks[mapping], jnp.max(scores, axis=-1))
            correction = jnp.exp(peaks[mapping] - peak)
            expo = jnp.exp(scores - peak[..., None])
            new_totals.append(totals[mapping] * correction + jnp.sum(expo, axis=-1))
            gained = jnp.einsum(
                "kgbt,tke->bkge",
                expo.astype(jnp.bfloat16),
                value_three,
                preferred_element_type=jnp.float32,
            )
            new_attends.append(
                attends[mapping] * jnp.transpose(correction, (2, 0, 1))[..., None] + gained
            )
            new_peaks.append(peak)
        return (jnp.stack(new_peaks), jnp.stack(new_totals), jnp.stack(new_attends))

    peaks, totals, attends = lax.cond(
        jnp.int32(0) <= last_position, update, lambda state: state, start_state
    )
    first = attends[0] / jnp.transpose(totals[0], (2, 0, 1))[..., None]
    second = attends[1] / jnp.transpose(totals[1], (2, 0, 1))[..., None]
    head_out = (first - lambdas[None, :, :, None] * second).reshape(row_count, heads_local, DV)
    normed = (
        head_out
        * lax.rsqrt(jnp.mean(head_out * head_out, axis=-1, keepdims=True) + norm_eps)
        * head_gain
    )
    attend_out = normed.astype(jnp.bfloat16).reshape(row_count, heads_local * DV)
    recur_rows, attend_rows = (
        lax.all_to_all(recur_out, "tp", split_axis=0, concat_axis=1, tiled=True),
        lax.all_to_all(attend_out, "tp", split_axis=0, concat_axis=1, tiled=True),
    )
    whole_recur, whole_attend = in_one_piece((w_out_recur, w_out_attend), "tp", 0, 1)
    merged = jnp.dot(recur_rows, whole_recur, preferred_element_type=jnp.float32) + jnp.dot(
        attend_rows, whole_attend, preferred_element_type=jnp.float32
    )
    final = (
        merged * lax.rsqrt(jnp.mean(merged * merged, axis=1, keepdims=True) + norm_eps) * out_gain
    )
    return final.astype(jnp.bfloat16)


def solution(mesh):
    in_specs = (
        P(("fs", "sp"), "tp"),
        P(),
        P(None, "tp"),
        P(None, "tp"),
        P("tp", None, None),
        P("tp", None, None),
        P("tp"),
        P(("fs", "sp"), "tp"),
        P(None, "tp"),
        P(None, "tp"),
        P(None, "tp"),
        P("tp"),
        P(),
        P("tp", None),
        P("tp", None),
        P(),
    )
    out_specs = P(("fs", "sp", "tp"), None)
    return jax.shard_map(body, mesh=mesh, in_specs=in_specs, out_specs=out_specs, check_vma=False)
```

profile of v0, /device:TPU:1, one launch (start us, length us, event | category | flops | bytes accessed | tf_op | source)
XLA Modules:
  0.0 134.3 jit_solution(11392075129574978183)
XLA Ops:
  6.5 5.3 %all_gather.9 = bf16[128,2048]{1,0:T(8,128)(2,1)S(1)} all-gather(bf16[128,1024]{1,0:T(8,128)(2,1)} %param.18), channel_id=1, replica_groups=mesh['sp'=32,'fs'=4,'tp'=2] {'tp'}, dimensions={1}, use_global_device_ids=true | all-gather | bytes 786432 | tf_op jit(solution)/shard_map/all_gather | solution.py:99
  12.1 3.3 %fusion.51 = bf16[128,1280]{1,0:T(8,128)(2,1)S(1)} fusion(bf16[2048,128]{1,0:T(8,128)(2,1)} %param.28, bf16[2048,128]{1,0:T(8,128)(2,1)} %param.27, bf16[2048,512]{1,0:T(8,128)(2,1)} %param.26, bf16[2048,512]{1,0:T(8,128)(2,1)} %param.20, bf16[128,2048]{1,0:T(8,128)(2,1)S(1)} %all_gather.9, f32[2048]{0:T(1024)} %param.19, f32[128]{0:T(128)S(1)} %add_rsqrt_fusion.2), kind=kOutput, calls=%fused_computation.54 | convolution fusion | flops 693174272 | bytes 6103552 | tf_op jit(solution)/shard_map/dot_general | solution.py:101
  15.4 0.6 concatenate.68
  16.2 1.6 %collective-permute-start = (bf16[3,512]{1,0:T(4,128)(2,1)S(1)}, bf16[3,512]{1,0:T(4,128)(2,1)S(1)}, u32[]{:S(2)}, u32[]{:S(2)}) collective-permute-start(bf16[3,512]{1,0:T(4,128)(2,1)S(1)} %slice.456), channel_id=1, source_target_pairs={{0,8},{8,16},{16,24},{24,32},{32,40},{40,48},{48,56},{56,64},{64,7... | collective-permute-start | bytes 9224 | tf_op jit(solution)/shard_map/ppermute | solution.py:16
  17.8 4.0 %pad_maximum_fusion.2 = bf16[512,4096]{1,0:T(8,128)(2,1)} fusion(bf16[512,2048]{1,0:T(8,128)(2,1)S(1)} %copy-done.2, bf16[512,2048]{1,0:T(8,128)(2,1)} %param.31), kind=kLoop, calls=%fused_computation.52 | loop fusion | flops 8388608 | bytes 8388608 | tf_op jit(solution)/shard_map/concatenate | solution.py:64
  26.5 0.7 broadcast_in_dim.59
  27.2 10.9 %all-to-all-start = ((f32[32,2,512]{2,1,0:T(2,128)}), f32[32,2,512]{2,1,0:T(2,128)S(1)}, u32[]{:S(2)}, u32[]{:S(2)}) async-start(f32[32,2,512]{2,1,0:T(2,128)} %broadcast_in_dim.59), calls=%async_computation | async-start | bytes 262144 | tf_op jit(solution)/shard_map/all_to_all | solution.py:21
  38.3 9.3 %all-to-all-done = f32[32,2,512]{2,1,0:T(2,128)S(1)} async-done(((f32[32,2,512]{2,1,0:T(2,128)}), f32[32,2,512]{2,1,0:T(2,128)S(1)}, u32[]{:S(2)}, u32[]{:S(2)}) %all-to-all-start) | async-done | bytes 131104 | tf_op jit(solution)/shard_map/all_to_all | solution.py:21
  48.3 5.4 %all_to_all.40 = bf16[2,64,512]{2,1,0:T(8,128)(2,1)S(1)} all-to-all(bf16[2,64,512]{2,1,0:T(8,128)(2,1)S(1)} %bitcast.173), channel_id=1, replica_groups=mesh['sp'=32,'fs'=4,'tp'=2] {'tp'}, dimensions={0} | all-to-all | bytes 262144 | tf_op jit(solution)/shard_map/all_to_all | solution.py:193
  53.7 37.1 %all-gather.5.cloned.1.call-done = bf16[4096,256]{1,0:T(8,128)(2,1)} async-done(((bf16[128,256]{1,0:T(8,128)(2,1)}), bf16[4096,256]{1,0:T(8,128)(2,1)}) %all-gather.5.cloned.1.call-update) | async-done | bytes 2097168 | tf_op jit(solution)/shard_map/all_gather | solution.py:65
  90.8 10.7 %conditional.1 = (f32[2,1,4,128]{3,2,1,0:T(4,128)S(1)}, f32[2,128,1,4,128]{4,1,3,2,0:T(8,128)S(1)}) conditional(s32[]{:T(128)} %convert_element_type.45, () %tuple.13, (s32[]{:T(128)}, s32[128]{0:T(128)S(1)}, bf16[4096,256]{1,0:T(8,128)(2,1)}, bf16[128,1280]{1,0:T(8,128)(2,1)S(1)}) %tuple.14), branch_computations={%region_1.2_spmd, %region_2.7_spmd} | conditional | flops 1640763520 | bytes 70309424 | solution.py:180
  91.1 1.3 slice.238
  92.4 0.5 copy.45
  93.3 1.3 fusion.88
  94.6 1.1 fusion.1
  95.7 1.3 fusion.87
  97.0 1.1 fusion.3
  98.2 1.6 %fusion.21 = f32[1,128,1,4,128]{4,1,3,2,0:T(8,128)S(1)} fusion(f32[1,4,128,4096]{2,3,1,0:T(8,128)S(1)} %get-tuple-element.41, f32[4,128]{1,0:T(4,128)S(1)} %broadcast_maximum_fusion, bf16[4096,256]{1,0:T(8,128)(2,1)S(1)} %copy-done.1, f32[128,4]{0,1:T(4,128)S(1)} %get-tuple-element.45), kind=kOutput, calls=%fused_computation.18 | convolution fusion | flops 541130752 | bytes 9703424 | tf_op jit(solution)/shard_map/cond/branch_1_fun/kgbt,tke->bkge/dot_general | solution.py:168
  99.8 1.6 %fusion.27 = f32[1,128,1,4,128]{4,1,3,2,0:T(8,128)S(1)} fusion(f32[1,4,128,4096]{2,3,1,0:T(8,128)S(1)} %get-tuple-element.43, f32[4,128]{1,0:T(4,128)S(1)} %broadcast_maximum_fusion.1, bf16[4096,256]{1,0:T(8,128)(2,1)S(1)} %copy-done.1, f32[128,4]{0,1:T(4,128)S(1)} %get-tuple-element.36), kind=kOutput, calls=%fused_computation.20 | convolution fusion | flops 541130752 | bytes 9703424 | tf_op jit(solution)/shard_map/cond/branch_1_fun/kgbt,tke->bkge/dot_general | solution.py:168
  103.9 9.0 %all_to_all.41 = bf16[2,64,512]{2,1,0:T(8,128)(2,1)S(1)} all-to-all(bf16[2,64,512]{2,1,0:T(8,128)(2,1)S(1)} %multiply_convert_fusion.1), channel_id=1, replica_groups=mesh['sp'=32,'fs'=4,'tp'=2] {'tp'}, dimensions={0} | all-to-all | bytes 262144 | tf_op jit(solution)/shard_map/all_to_all | solution.py:194
  112.9 7.5 %all-gather.3.cloned.1.call-done = bf16[1024,4096]{1,0:T(8,128)(2,1)} async-done(((bf16[512,4096]{1,0:T(8,128)(2,1)}), bf16[1024,4096]{1,0:T(8,128)(2,1)}) %all-gather.3.cloned.1.call-update) | async-done | bytes 8388624 | tf_op jit(solution)/shard_map/all_gather | solution.py:65
  120.4 3.0 %fusion.44 = f32[64,2048]{1,0:T(8,128)S(1)} fusion(bf16[64,1024]{1,0:T(8,128)(2,1)S(1)} %bitcast.180, bf16[1024,4096]{1,0:T(8,128)(2,1)} %all-gather.3.cloned.1.call-done), kind=kOutput, calls=%fused_computation.48 | convolution fusion | flops 268435456 | bytes 4849664 | tf_op jit(solution)/shard_map/dot_general | solution.py:197
  123.4 3.2 %multiply_reduce_fusion = (f32[64]{0:T(128)S(1)}, f32[64,2048]{1,0:T(8,128)S(1)}) fusion(f32[64,2048]{1,0:T(8,128)S(1)} %fusion.44, bf16[64,1024]{1,0:T(8,128)(2,1)S(1)} %bitcast.172, bf16[1024,4096]{1,0:T(8,128)(2,1)} %all-gather.3.cloned.1.call-done), kind=kOutput, calls=%fused_computation.69 | convolution fusion | flops 268828608 | bytes 5374208 | tf_op jit(solution)/shard_map/dot_general | solution.py:197
  126.6 0.8 multiply_convert_fusion
  (204 shorter events, 8.0 us)
Async XLA Ops:
  6.5 15.8 %copy-start = (bf16[8,64,64]{2,1,0:T(8,128)(2,1)S(1)}, bf16[8,64,64]{2,1,0:T(8,128)(2,1)}, u32[]{:S(2)}) copy-start(bf16[8,64,64]{2,1,0:T(8,128)(2,1)} %param.23) | copy-start | bytes 196612
  6.5 84.3 %all-gather.5.cloned.1.call-start = ((), (), s32[]{:S(2)}) async-start(), calls=%async_computation.4 | async-start | bytes 2162688 | tf_op jit(solution)/shard_map/all_gather | solution.py:65
  12.1 5.7 %copy-start.2 = (bf16[512,2048]{1,0:T(8,128)(2,1)S(1)}, bf16[512,2048]{1,0:T(8,128)(2,1)}, u32[]{:S(2)}) copy-start(bf16[512,2048]{1,0:T(8,128)(2,1)} %param.32) | copy-start | bytes 6291460
  15.4 6.4 %copy-start.4 = (f32[4,512]{1,0:T(4,128)S(1)}, f32[4,512]{1,0:T(4,128)}, u32[]{:S(2)}) copy-start(f32[4,512]{1,0:T(4,128)} %param.21) | copy-start | bytes 24580
  15.4 6.4 %copy-start.7 = (f32[512]{0:T(512)S(1)}, f32[512]{0:T(512)}, u32[]{:S(2)}) copy-start(f32[512]{0:T(512)} %param.24) | copy-start | bytes 6148
  15.4 6.4 %copy-start.5 = (f32[128,8]{0,1:T(8,128)S(1)}, f32[128,8]{0,1:T(8,128)}, u32[]{:S(2)}) copy-start(f32[128,8]{0,1:T(8,128)} %param.25) | copy-start | bytes 12292
  16.1 104.3 %all-gather.3.cloned.1.call-start = ((), (), s32[]{:S(2)}) async-start(), calls=%async_computation.3 | async-start | bytes 12582912 | tf_op jit(solution)/shard_map/all_gather | solution.py:65
  16.2 6.6 %copy-start.9 = (bf16[8,64,64]{2,1,0:T(8,128)(2,1)S(1)}, bf16[8,64,64]{2,1,0:T(8,128)(2,1)}, u32[]{:S(2)}) copy-start(bf16[8,64,64]{2,1,0:T(8,128)(2,1)} %param.22) | copy-start | bytes 196612
  16.2 5.9 %collective-permute-start = (bf16[3,512]{1,0:T(4,128)(2,1)S(1)}, bf16[3,512]{1,0:T(4,128)(2,1)S(1)}, u32[]{:S(2)}, u32[]{:S(2)}) collective-permute-start(bf16[3,512]{1,0:T(4,128)(2,1)S(1)} %slice.456), channel_id=1, source_target_pairs={{0,8},{8,16},{16,24},{24,32},{32,40},{40,48},{48,56},{56,64},{64,7... | collective-permute-start | bytes 9224 | tf_op jit(solution)/shard_map/ppermute | solution.py:16
  22.8 15.4 %copy-start.6 = (f32[4]{0:T(128)S(1)}, f32[4]{0:T(128)}, u32[]{:S(2)}) copy-start(f32[4]{0:T(128)} %param.29) | copy-start | bytes 52
  22.8 15.4 %copy-start.8 = (f32[128]{0:T(128)S(1)}, f32[128]{0:T(128)}, u32[]{:S(2)}) copy-start(f32[128]{0:T(128)} %param.30) | copy-start | bytes 1540
  27.2 20.4 %all-to-all-start = ((f32[32,2,512]{2,1,0:T(2,128)}), f32[32,2,512]{2,1,0:T(2,128)S(1)}, u32[]{:S(2)}, u32[]{:S(2)}) async-start(f32[32,2,512]{2,1,0:T(2,128)} %broadcast_in_dim.59), calls=%async_computation | async-start | bytes 262144 | tf_op jit(solution)/shard_map/all_to_all | solution.py:21
  95.7 2.5 %copy-start.1 = (bf16[4096,256]{1,0:T(8,128)(2,1)S(1)}, bf16[4096,256]{1,0:T(8,128)(2,1)}, u32[]{:S(2)}) copy-start(bf16[4096,256]{1,0:T(8,128)(2,1)} %get-tuple-element.22) | copy-start | bytes 6291460 | tf_op jit(solution)/shard_map/cond
  102.5 24.1 %copy-start.3 = (f32[2048]{0:T(1024)S(1)}, f32[2048]{0:T(1024)}, u32[]{:S(2)}) copy-start(f32[2048]{0:T(1024)} %param.33) | copy-start | bytes 24580
Sparse Core Ops, SparseCore 0:
  16.2 74.5 all-gather.4
  92.6 27.7 all-gather.2
where the time goes:
time: 135 us; the launch traced here: 134 us
  waiting for transfers between devices  54 us (40%)
  blocking collectives  19.7 us (15%)
  matrix products  15.9 us (12%)
  between operations  14.4 us (11%)
  starting transfers between devices  12.6 us (9%)
  other arithmetic  9.36 us (7%)
  local copies, waits for them, and re-layouts  8.21 us (6%)
    all_gather x2, waiting for transfers between devices, in_one_piece(): result, at, outs = (lax.all_gather(both, axis, axis=dim, tiled=True), 0, [])  44.6 us
    all_to_all x1, starting transfers between devices, copy_for_each(): return lax.all_to_all(copies, axis, split_axis=0, concat_axis=0, tiled=True)  10.9 us
    all_to_all x1, waiting for transfers between devices, copy_for_each(): return lax.all_to_all(copies, axis, split_axis=0, concat_axis=0, tiled=True)  9.34 us
    all_to_all x1, blocking collectives, body(): lax.all_to_all(attend_out, 'tp', split_axis=0, concat_axis=1, tiled=True)  8.96 us
    all_to_all x1, blocking collectives, body(): lax.all_to_all(recur_out, 'tp', split_axis=0, concat_axis=1, tiled=True)  5.39 us
    all_gather x1, blocking collectives, body(): lax.all_gather(tokens, 'tp', axis=1, tiled=True).astype(jnp.float32)  5.34 us
    concatenate x1, other arithmetic, in_one_piece(): both = jnp.concatenate(arrays, axis=along)  3.96 us
    dot_general x1, matrix products, body(): accum = jnp.dot(scaled, all_weights, preferred_element_type=jnp.float32)  3.32 us
  transfers between devices with their start and end apart: 4, of which 3 were waited for; matrix products, arithmetic and copies ran while one was open for 17% of the time, Pallas kernels for 0%

commit v1 on v0

--- a/solution.py
+++ b/solution.py
@@ -96,7 +96,9 @@
     query_cols = w_query.shape[1]
     key_cols = w_key.shape[1]
     all_weights = jnp.concatenate([w_recur_in, w_query, w_key, w_value], axis=1)
-    wide_piece = lax.all_gather(tokens, "tp", axis=1, tiled=True).astype(jnp.float32)
+    wide_piece = jnp.concatenate(
+        lax.all_to_all(jnp.stack([tokens] * lax.axis_size("tp")), "tp", 0, 0), axis=1
+    ).astype(jnp.float32)
     scaled = (wide_piece * norm_gain).astype(jnp.bfloat16)
     accum = jnp.dot(scaled, all_weights, preferred_element_type=jnp.float32)
     squares = jnp.sum(wide_piece * wide_piece, axis=1, keepdims=True)

time: 135 us -> 139 us (1.030)
  blocking collectives: 19.7 us -> 21.3 us
    all_to_all x0 -> x1, blocking collectives: none -> 6.98 us  [body(): lax.all_to_all(jnp.stack([tokens] * lax.axis_size('tp')), 'tp', 0, 0)]
    all_gather x1 -> x0, blocking collectives: 5.34 us -> none  [body(): lax.all_gather(tokens, 'tp', axis=1, tiled=True).astype(jnp.float32)]
  transfers between devices with their start and end apart: 4 -> 4, of which waited for: 3 -> 3; matrix products, arithmetic and copies ran while one was open for 17% -> 16% of each run, Pallas kernels for 0% -> 0%
where the time goes in v1:
time: 139 us; the launch traced here: 138 us
  waiting for transfers between devices  54 us (39%)
  blocking collectives  21.3 us (15%)
  matrix products  15.9 us (11%)
  between operations  14.5 us (10%)
  starting transfers between devices  12.6 us (9%)
  other arithmetic  10.5 us (8%)
  local copies, waits for them, and re-layouts  9.37 us (7%)
    all_gather x2, waiting for transfers between devices, in_one_piece(): result, at, outs = (lax.all_gather(both, axis, axis=dim, tiled=True), 0, [])  44.6 us
    all_to_all x1, starting transfers between devices, copy_for_each(): return lax.all_to_all(copies, axis, split_axis=0, concat_axis=0, tiled=True)  10.9 us
    all_to_all x1, waiting for transfers between devices, copy_for_each(): return lax.all_to_all(copies, axis, split_axis=0, concat_axis=0, tiled=True)  9.28 us
    all_to_all x1, blocking collectives, body(): lax.all_to_all(attend_out, 'tp', split_axis=0, concat_axis=1, tiled=True)  8.96 us
    all_to_all x1, blocking collectives, body(): lax.all_to_all(jnp.stack([tokens] * lax.axis_size('tp')), 'tp', 0, 0)  6.98 us
    all_to_all x1, blocking collectives, body(): lax.all_to_all(recur_out, 'tp', split_axis=0, concat_axis=1, tiled=True)  5.4 us
    concatenate x1, other arithmetic, in_one_piece(): both = jnp.concatenate(arrays, axis=along)  3.96 us
    dot_general x1, matrix products, body(): accum = jnp.dot(scaled, all_weights, preferred_element_type=jnp.float32)  3.31 us
  transfers between devices with their start and end apart: 4, of which 3 were waited for; matrix products, arithmetic and copies ran while one was open for 16% of the time, Pallas kernels for 0%

profile of v1, /device:TPU:1, one launch (start us, length us, event | category | flops | bytes accessed | tf_op | source)
XLA Modules:
  0.0 138.3 jit_solution(9746811293464727093)
XLA Ops:
  6.5 1.2 copy.51
  7.7 7.0 %all_to_all.45 = bf16[2,128,1024]{1,2,0:T(8,128)(2,1)S(1)} all-to-all(bf16[2,128,1024]{1,2,0:T(8,128)(2,1)S(1)} %pad_maximum_fusion.3), channel_id=1, replica_groups=mesh['sp'=32,'fs'=4,'tp'=2] {'tp'}, dimensions={0} | all-to-all | bytes 1048576 | tf_op jit(solution)/shard_map/all_to_all | solution.py:100
  15.0 1.0 fusion.63
  16.1 3.3 %fusion.51 = bf16[128,1280]{1,0:T(8,128)(2,1)S(1)} fusion(bf16[128,2048]{0,1:T(8,128)(2,1)S(1)} %fusion.63, bf16[2048,128]{1,0:T(8,128)(2,1)} %param.28, bf16[2048,128]{1,0:T(8,128)(2,1)} %param.27, bf16[2048,512]{1,0:T(8,128)(2,1)} %param.26, bf16[2048,512]{1,0:T(8,128)(2,1)} %param.20, f32[128]{0:T(128)S(1)} %add_rsqrt_fusion.2), kind=kOutput, calls=%fused_computation.54 | convolution fusion | flops 692387840 | bytes 6095360 | tf_op jit(solution)/shard_map/dot_general | solution.py:103
  20.1 1.6 %collective-permute-start = (bf16[3,512]{1,0:T(4,128)(2,1)S(1)}, bf16[3,512]{1,0:T(4,128)(2,1)S(1)}, u32[]{:S(2)}, u32[]{:S(2)}) collective-permute-start(bf16[3,512]{1,0:T(4,128)(2,1)S(1)} %slice.456), channel_id=1, source_target_pairs={{0,8},{8,16},{16,24},{24,32},{32,40},{40,48},{48,56},{56,64},{64,7... | collective-permute-start | bytes 9224 | tf_op jit(solution)/shard_map/ppermute | solution.py:16
  21.8 4.0 %pad_maximum_fusion.2 = bf16[512,4096]{1,0:T(8,128)(2,1)} fusion(bf16[512,2048]{1,0:T(8,128)(2,1)S(1)} %copy-done.2, bf16[512,2048]{1,0:T(8,128)(2,1)} %param.31), kind=kLoop, calls=%fused_computation.52 | loop fusion | flops 8388608 | bytes 8388608 | tf_op jit(solution)/shard_map/concatenate | solution.py:64
  30.5 0.7 broadcast_in_dim.59
  31.2 10.9 %all-to-all-start.1 = ((f32[32,2,512]{2,1,0:T(2,128)}), f32[32,2,512]{2,1,0:T(2,128)S(1)}, u32[]{:S(2)}, u32[]{:S(2)}) async-start(f32[32,2,512]{2,1,0:T(2,128)} %broadcast_in_dim.59), calls=%async_computation.1 | async-start | bytes 262144 | tf_op jit(solution)/shard_map/all_to_all | solution.py:21
  42.2 9.3 %all-to-all-done.1 = f32[32,2,512]{2,1,0:T(2,128)S(1)} async-done(((f32[32,2,512]{2,1,0:T(2,128)}), f32[32,2,512]{2,1,0:T(2,128)S(1)}, u32[]{:S(2)}, u32[]{:S(2)}) %all-to-all-start.1) | async-done | bytes 131104 | tf_op jit(solution)/shard_map/all_to_all | solution.py:21
  52.2 5.4 %all_to_all.46 = bf16[2,64,512]{2,1,0:T(8,128)(2,1)S(1)} all-to-all(bf16[2,64,512]{2,1,0:T(8,128)(2,1)S(1)} %bitcast.182), channel_id=1, replica_groups=mesh['sp'=32,'fs'=4,'tp'=2] {'tp'}, dimensions={0} | all-to-all | bytes 262144 | tf_op jit(solution)/shard_map/all_to_all | solution.py:195
  57.6 37.2 %all-gather.5.cloned.1.call-done = bf16[4096,256]{1,0:T(8,128)(2,1)} async-done(((bf16[128,256]{1,0:T(8,128)(2,1)}), bf16[4096,256]{1,0:T(8,128)(2,1)}) %all-gather.5.cloned.1.call-update) | async-done | bytes 2097168 | tf_op jit(solution)/shard_map/all_gather | solution.py:65
  94.8 10.7 %conditional.1 = (f32[2,1,4,128]{3,2,1,0:T(4,128)S(1)}, f32[2,128,1,4,128]{4,1,3,2,0:T(8,128)S(1)}) conditional(s32[]{:T(128)} %convert_element_type.58, () %tuple.13, (s32[]{:T(128)}, s32[128]{0:T(128)S(1)}, bf16[4096,256]{1,0:T(8,128)(2,1)}, bf16[128,1280]{1,0:T(8,128)(2,1)S(1)}) %tuple.14), branch_computations={%region_1.2_spmd, %region_2.7_spmd} | conditional | flops 1640763520 | bytes 70309424 | solution.py:182
  95.0 1.3 slice.238
  97.2 1.3 fusion.85
  98.5 1.1 fusion.1
  99.7 1.3 fusion.84
  101.0 1.1 fusion.3
  102.2 1.6 %fusion.21 = f32[1,128,1,4,128]{4,1,3,2,0:T(8,128)S(1)} fusion(f32[1,4,128,4096]{2,3,1,0:T(8,128)S(1)} %get-tuple-element.41, f32[4,128]{1,0:T(4,128)S(1)} %broadcast_maximum_fusion, bf16[4096,256]{1,0:T(8,128)(2,1)S(1)} %copy-done.1, f32[128,4]{0,1:T(4,128)S(1)} %get-tuple-element.45), kind=kOutput, calls=%fused_computation.18 | convolution fusion | flops 541130752 | bytes 9703424 | tf_op jit(solution)/shard_map/cond/branch_1_fun/kgbt,tke->bkge/dot_general | solution.py:170
  103.8 1.6 %fusion.27 = f32[1,128,1,4,128]{4,1,3,2,0:T(8,128)S(1)} fusion(f32[1,4,128,4096]{2,3,1,0:T(8,128)S(1)} %get-tuple-element.43, f32[4,128]{1,0:T(4,128)S(1)} %broadcast_maximum_fusion.1, bf16[4096,256]{1,0:T(8,128)(2,1)S(1)} %copy-done.1, f32[128,4]{0,1:T(4,128)S(1)} %get-tuple-element.36), kind=kOutput, calls=%fused_computation.20 | convolution fusion | flops 541130752 | bytes 9703424 | tf_op jit(solution)/shard_map/cond/branch_1_fun/kgbt,tke->bkge/dot_general | solution.py:170
  107.9 9.0 %all_to_all.47 = bf16[2,64,512]{2,1,0:T(8,128)(2,1)S(1)} all-to-all(bf16[2,64,512]{2,1,0:T(8,128)(2,1)S(1)} %multiply_convert_fusion.1), channel_id=1, replica_groups=mesh['sp'=32,'fs'=4,'tp'=2] {'tp'}, dimensions={0} | all-to-all | bytes 262144 | tf_op jit(solution)/shard_map/all_to_all | solution.py:196
  116.9 7.5 %all-gather.3.cloned.1.call-done = bf16[1024,4096]{1,0:T(8,128)(2,1)} async-done(((bf16[512,4096]{1,0:T(8,128)(2,1)}), bf16[1024,4096]{1,0:T(8,128)(2,1)}) %all-gather.3.cloned.1.call-update) | async-done | bytes 8388624 | tf_op jit(solution)/shard_map/all_gather | solution.py:65
  124.4 3.0 %fusion.44 = f32[64,2048]{1,0:T(8,128)S(1)} fusion(bf16[64,1024]{1,0:T(8,128)(2,1)S(1)} %bitcast.189, bf16[1024,4096]{1,0:T(8,128)(2,1)} %all-gather.3.cloned.1.call-done), kind=kOutput, calls=%fused_computation.48 | convolution fusion | flops 268435456 | bytes 4849664 | tf_op jit(solution)/shard_map/dot_general | solution.py:199
  127.4 3.2 %multiply_reduce_fusion.1 = (f32[64]{0:T(128)S(1)}, f32[64,2048]{1,0:T(8,128)S(1)}) fusion(f32[64,2048]{1,0:T(8,128)S(1)} %fusion.44, bf16[64,1024]{1,0:T(8,128)(2,1)S(1)} %bitcast.181, bf16[1024,4096]{1,0:T(8,128)(2,1)} %all-gather.3.cloned.1.call-done), kind=kOutput, calls=%fused_computation.69 | convolution fusion | flops 268828608 | bytes 5374208 | tf_op jit(solution)/shard_map/dot_general | solution.py:199
  130.6 0.8 multiply_convert_fusion
  (207 shorter events, 9.3 us)
Async XLA Ops:
  6.5 19.8 %copy-start = (bf16[8,64,64]{2,1,0:T(8,128)(2,1)S(1)}, bf16[8,64,64]{2,1,0:T(8,128)(2,1)}, u32[]{:S(2)}) copy-start(bf16[8,64,64]{2,1,0:T(8,128)(2,1)} %param.23) | copy-start | bytes 196612
  6.5 88.3 %all-gather.5.cloned.1.call-start = ((), (), s32[]{:S(2)}) async-start(), calls=%async_computation.5 | async-start | bytes 2162688 | tf_op jit(solution)/shard_map/all_gather | solution.py:65
  16.1 5.7 %copy-start.2 = (bf16[512,2048]{1,0:T(8,128)(2,1)S(1)}, bf16[512,2048]{1,0:T(8,128)(2,1)}, u32[]{:S(2)}) copy-start(bf16[512,2048]{1,0:T(8,128)(2,1)} %param.32) | copy-start | bytes 6291460
  19.4 6.4 %copy-start.4 = (f32[4,512]{1,0:T(4,128)S(1)}, f32[4,512]{1,0:T(4,128)}, u32[]{:S(2)}) copy-start(f32[4,512]{1,0:T(4,128)} %param.21) | copy-start | bytes 24580
  19.4 6.4 %copy-start.7 = (f32[512]{0:T(512)S(1)}, f32[512]{0:T(512)}, u32[]{:S(2)}) copy-start(f32[512]{0:T(512)} %param.24) | copy-start | bytes 6148
  19.4 6.4 %copy-start.5 = (f32[128,8]{0,1:T(8,128)S(1)}, f32[128,8]{0,1:T(8,128)}, u32[]{:S(2)}) copy-start(f32[128,8]{0,1:T(8,128)} %param.25) | copy-start | bytes 12292
  20.1 104.3 %all-gather.3.cloned.1.call-start = ((), (), s32[]{:S(2)}) async-start(), calls=%async_computation.4 | async-start | bytes 12582912 | tf_op jit(solution)/shard_map/all_gather | solution.py:65
  20.1 6.6 %copy-start.9 = (bf16[8,64,64]{2,1,0:T(8,128)(2,1)S(1)}, bf16[8,64,64]{2,1,0:T(8,128)(2,1)}, u32[]{:S(2)}) copy-start(bf16[8,64,64]{2,1,0:T(8,128)(2,1)} %param.22) | copy-start | bytes 196612
  20.1 5.9 %collective-permute-start = (bf16[3,512]{1,0:T(4,128)(2,1)S(1)}, bf16[3,512]{1,0:T(4,128)(2,1)S(1)}, u32[]{:S(2)}, u32[]{:S(2)}) collective-permute-start(bf16[3,512]{1,0:T(4,128)(2,1)S(1)} %slice.456), channel_id=1, source_target_pairs={{0,8},{8,16},{16,24},{24,32},{32,40},{40,48},{48,56},{56,64},{64,7... | collective-permute-start | bytes 9224 | tf_op jit(solution)/shard_map/ppermute | solution.py:16
  26.8 15.4 %copy-start.6 = (f32[4]{0:T(128)S(1)}, f32[4]{0:T(128)}, u32[]{:S(2)}) copy-start(f32[4]{0:T(128)} %param.29) | copy-start | bytes 52
  26.8 15.4 %copy-start.8 = (f32[128]{0:T(128)S(1)}, f32[128]{0:T(128)}, u32[]{:S(2)}) copy-start(f32[128]{0:T(128)} %param.30) | copy-start | bytes 1540
  31.2 20.3 %all-to-all-start.1 = ((f32[32,2,512]{2,1,0:T(2,128)}), f32[32,2,512]{2,1,0:T(2,128)S(1)}, u32[]{:S(2)}, u32[]{:S(2)}) async-start(f32[32,2,512]{2,1,0:T(2,128)} %broadcast_in_dim.59), calls=%async_computation.1 | async-start | bytes 262144 | tf_op jit(solution)/shard_map/all_to_all | solution.py:21
  99.7 2.5 %copy-start.1 = (bf16[4096,256]{1,0:T(8,128)(2,1)S(1)}, bf16[4096,256]{1,0:T(8,128)(2,1)}, u32[]{:S(2)}) copy-start(bf16[4096,256]{1,0:T(8,128)(2,1)} %get-tuple-element.22) | copy-start | bytes 6291460 | tf_op jit(solution)/shard_map/cond
  106.5 24.1 %copy-start.3 = (f32[2048]{0:T(1024)S(1)}, f32[2048]{0:T(1024)}, u32[]{:S(2)}) copy-start(f32[2048]{0:T(1024)} %param.33) | copy-start | bytes 24580
Sparse Core Ops, SparseCore 0:
  20.2 74.5 all-gather.4
  96.6 27.7 all-gather.2
